TPU v7x, 256 devices: a 4x2x16 block of a 4x16x16 slice. The times are simulated.
256 devices in a mesh: grp: 2 (over y), ep: 32 (over z, core), tp: 4 (over x).
Axes of the slice: x: 4, y: 2, z: 16, core: 2. Of those that a mesh axis runs over, the one named last changes fastest.
The devices are a block of a 4x16x16 slice.
Arguments:
- outer_gate: bfloat16 [16384, 2048], P(('grp', 'ep'), 'tp'), parts along dimension 0, may hold values from -6 to 6
- inner_gate: bfloat16 [16384, 2048], P(('grp', 'ep'), 'tp'), parts along dimension 0, may hold values from -6 to 6
- inner_value: bfloat16 [16384, 2048], P(('grp', 'ep'), 'tp'), parts along dimension 0, may hold values from -6 to 6
- conv_taps: bfloat16 [3, 2048], replicated, may hold values from -3 to 3
- mixer_out: bfloat16 [2048, 2048], P('tp'), may hold values from -0.125 to 0.125
- mixer_gain: float32 [2048], replicated, may hold values from 0.1 to 1.9
- moe_tokens: bfloat16 [16384, 2048], P(('grp', 'ep', 'tp')), parts along dimension 0, may hold values from -6 to 6
- expert_gain: float32 [2048], replicated, may hold values from 0.1 to 1.9
- route_ids: int32 [16384, 4], P(('grp', 'ep', 'tp')), parts along dimension 0, may hold values from 0 to 127, all different within a row; in each aligned block of 64 rows (0 to 63, 64 to 127, ...) at most 3 rows name the same one
- route_weights: float32 [16384, 4], P(('grp', 'ep', 'tp')), parts along dimension 0, may hold values from 0.2 to 1
- expert_gate: bfloat16 [128, 2048, 512], P(('ep', 'tp')), may hold values from -0.125 to 0.125
- expert_up: bfloat16 [128, 2048, 512], P(('ep', 'tp')), may hold values from -0.125 to 0.125
- expert_down: bfloat16 [128, 512, 2048], P(('ep', 'tp')), may hold values from -0.25 to 0.25
- shared_gate: bfloat16 [2048, 512], P(None, 'tp'), may hold values from -0.125 to 0.125
- shared_up: bfloat16 [2048, 512], P(None, 'tp'), may hold values from -0.125 to 0.125
- shared_down: bfloat16 [512, 2048], P('tp'), may hold values from -0.25 to 0.25
Outputs:
- mixed_rows: bfloat16 [16384, 2048], P(('grp', 'ep', 'tp')), parts along dimension 0
- expert_rows: bfloat16 [16384, 2048], P(('grp', 'ep', 'tp')), parts along dimension 0
There are 2 independent parts, one for each index of `grp`. A program takes and returns all parts, laid end to end along the dimension named above; an argument that names none is the same for every part. Nothing has to cross between parts.
Inputs may be any that keep to these rules, and one draw needn't show every extreme that they name: `route_ids`: each row names 4 different experts; among the 64 rows of one device (aligned blocks) no expert is named more than 3 times, a bound that some block reaches.
All inputs are finite; a program needn't handle non-finite values.
Results may differ from a plain program's by a relative error of at most 0.012.
Values may be sent and summed in bfloat16 or wider, within the bound.
No kernel may reach another device: no remote copies, remote signals or barrier semaphores. Data moves between devices by JAX's collectives and lax.ppermute only.
A program may use at most 64 MiB of HBM per device.

v0:
```python
import jax
import jax.numpy as jnp
from jax import lax
from jax.sharding import PartitionSpec as P

EPSILON = 1e-06


def passed_along(array, axis, by):
    size = lax.axis_size(axis)
    pairs = [(i, i + by) for i in range(size) if 0 <= i + by < size]
    return lax.ppermute(array, axis, pairs)


def laid_out(pieces, dim):
    shape = list(pieces.shape[1:])
    shape[dim] *= pieces.shape[0]
    return jnp.moveaxis(pieces, 0, dim).reshape(shape)


def work_in_pieces(array, axis, dim, apply, out_dim):
    size, span = (lax.axis_size(axis), array.shape[dim])
    count = 2 if span % 2 == 0 else 1
    outs, length = ([], span // count)
    for k in range(count):
        share = lax.slice_in_dim(array, k * length, (k + 1) * length, axis=dim)
        starts = jnp.arange(size) * span + k * length
        outs.append(jax.vmap(apply)(lax.all_gather(share, axis), starts))
    return laid_out(jnp.concatenate(outs, axis=out_dim + 1), out_dim)


def in_blocks(array, dim, size):
    shape = array.shape
    pieces = array.reshape(*shape[:dim], size, shape[dim] // size, *shape[dim + 1 :])
    return jnp.moveaxis(pieces, dim, 0)


def summed_on_arrival(array, axis, dim):
    pieces = in_blocks(array, dim, lax.axis_size(axis))
    arrived = lax.all_to_all(pieces, axis, split_axis=0, concat_axis=0, tiled=True)
    return arrived.astype(jnp.float32).sum(axis=0)


def rms_scale(values, gains):
    return values * lax.rsqrt(jnp.mean(values * values, axis=-1, keepdims=True) + EPSILON) * gains


def on_device(
    outer_gate,
    inner_gate,
    inner_value,
    conv_taps,
    mixer_out,
    mixer_gain,
    moe_tokens,
    expert_gain,
    route_ids,
    route_weights,
    expert_gate,
    expert_up,
    expert_down,
    shared_gate,
    shared_up,
    shared_down,
):
    columns = inner_gate.shape[1]
    kernel = lax.dynamic_slice_in_dim(conv_taps, lax.axis_index("tp") * columns, columns, 1).astype(
        jnp.float32
    )
    before_gate, before_value = passed_along((inner_gate[-2:], inner_value[-2:]), "ep", 1)
    gate_rows = jnp.concatenate([before_gate, inner_gate], axis=0).astype(jnp.float32)
    value_rows = jnp.concatenate([before_value, inner_value], axis=0).astype(jnp.float32)
    product = gate_rows * value_rows
    filtered = kernel[0] * product[:-2] + kernel[1] * product[1:-1] + kernel[2] * product[2:]
    scaled = (outer_gate.astype(jnp.float32) * filtered).astype(jnp.bfloat16)
    normed = rms_scale(moe_tokens.astype(jnp.float32), expert_gain).astype(jnp.bfloat16)
    feature_width = normed.shape[1]

    def shared_piece(piece, start):
        gate_value = jnp.dot(piece, shared_gate, preferred_element_type=jnp.float32)
        up_value = jnp.dot(piece, shared_up, preferred_element_type=jnp.float32)
        return (jax.nn.silu(gate_value) * up_value).astype(jnp.bfloat16)

    shared_act = work_in_pieces(normed, "tp", 0, shared_piece, 0)
    mixer_part = jnp.dot(scaled, mixer_out, preferred_element_type=jnp.float32)
    shared_part = jnp.dot(shared_act, shared_down, preferred_element_type=jnp.float32)
    both_sums = summed_on_arrival(
        jnp.concatenate([mixer_part, shared_part], axis=1).astype(jnp.bfloat16), "tp", 0
    )
    mixed_rows = rms_scale(both_sums[:, :feature_width], mixer_gain).astype(jnp.bfloat16)
    shared_out = both_sums[:, feature_width:]
    row_count, top_count = route_ids.shape
    ep_count = lax.axis_size("ep")
    tp_count = lax.axis_size("tp")
    expert_count = ep_count * tp_count
    capacity = (3 * row_count * top_count + 2 * expert_count - 1) // (2 * expert_count)
    flat_ids = route_ids.reshape(-1)
    onehot = (flat_ids[:, None] == jnp.arange(expert_count, dtype=jnp.int32)[None, :]).astype(
        jnp.int32
    )
    slot_rank = jnp.sum(
        (jnp.cumsum(onehot, axis=0, dtype=jnp.int32) - onehot) * onehot, axis=1, dtype=jnp.int32
    )
    target = flat_ids * capacity + slot_rank
    token_of = jnp.arange(flat_ids.shape[0], dtype=jnp.int32) // top_count
    slot_token = jnp.zeros((expert_count * capacity,), jnp.int32).at[target].set(token_of)
    outgoing = normed[slot_token].reshape(expert_count, capacity, feature_width)
    arrived = lax.all_to_all(outgoing, ("ep", "tp"), split_axis=0, concat_axis=0, tiled=True)
    flat_in = arrived.reshape(expert_count * capacity, feature_width)
    gate_value = jnp.dot(flat_in, expert_gate[0], preferred_element_type=jnp.float32)
    up_value = jnp.dot(flat_in, expert_up[0], preferred_element_type=jnp.float32)
    active = (jax.nn.silu(gate_value) * up_value).astype(jnp.bfloat16)
    result = jnp.dot(active, expert_down[0], preferred_element_type=jnp.float32).astype(
        jnp.bfloat16
    )
    returned = lax.all_to_all(
        result.reshape(expert_count, capacity, feature_width),
        ("ep", "tp"),
        split_axis=0,
        concat_axis=0,
        tiled=True,
    )
    picked = returned.reshape(expert_count * capacity, feature_width)[target].astype(jnp.float32)
    weights = route_weights.reshape(-1)
    routed = jnp.sum(
        (weights[:, None] * picked).reshape(row_count, top_count, feature_width), axis=1
    )
    expert_rows = (shared_out + routed).astype(jnp.bfloat16)
    return (mixed_rows, expert_rows)


def solution(mesh):
    return jax.shard_map(
        on_device,
        mesh=mesh,
        in_specs=(
            P(("grp", "ep"), "tp"),
            P(("grp", "ep"), "tp"),
            P(("grp", "ep"), "tp"),
            P(),
            P("tp", None),
            P(),
            P(("grp", "ep", "tp"), None),
            P(),
            P(("grp", "ep", "tp"), None),
            P(("grp", "ep", "tp"), None),
            P(("ep", "tp"), None, None),
            P(("ep", "tp"), None, None),
            P(("ep", "tp"), None, None),
            P(None, "tp"),
            P(None, "tp"),
            P("tp", None),
        ),
        out_specs=(P(("grp", "ep", "tp"), None), P(("grp", "ep", "tp"), None)),
        check_vma=False,
    )
```

profile of v0, /device:TPU:33, one launch (start us, length us, event | category | flops | bytes accessed | tf_op | source)
XLA Modules:
  0.0 299.8 jit_solution(3649183781875547081)
XLA Ops:
  0.6 0.0 copy-start
  0.6 0.8 broadcast_multiply_fusion
  1.5 0.8 copy.21
  2.2 0.1 eq.29
  2.4 0.1 eq.25
  2.5 1.1 fusion.20
  3.6 0.1 copy.20
  3.7 0.1 mul.154
  3.8 0.1 copy.23
  3.9 0.2 fusion.40
  4.2 0.2 fusion.42
  4.4 1.4 scatter_custom_fusion
  5.9 1.1 fusion.22
  6.9 3.1 %gather_fusion = bf16[384,2048]{1,0:T(8,128)(2,1)} fusion(bf16[64,2048]{1,0:T(8,128)(2,1)S(1)} %fusion.22, s32[1024]{0:T(1024)S(1)} %pad_clamp_fusion.1), kind=kCustom, calls=%fused_computation | custom fusion | bytes 3147264 | tf_op jit(solution)/shard_map/gather | solution.py:107
  10.0 5.1 %reshape.98 = bf16[128,3,2048]{2,1,0:T(4,128)(2,1)} reshape(bf16[384,2048]{1,0:T(8,128)(2,1)} %gather_fusion) | data formatting | bytes 3145728 | tf_op jit(solution)/shard_map/reshape | solution.py:107
  15.2 0.0 copy-start.3
  15.2 0.0 copy-start.4
  15.2 0.0 copy-start.1
  15.2 31.2 %all-to-all-start.1 = ((bf16[128,3,2048]{2,1,0:T(4,128)(2,1)}), bf16[128,3,2048]{2,1,0:T(4,128)(2,1)}, u32[]{:S(2)}, u32[]{:S(2)}) async-start(bf16[128,3,2048]{2,1,0:T(4,128)(2,1)} %reshape.98), calls=%async_computation.1 | async-start | bytes 4194304 | tf_op jit(solution)/shard_map/all_to_all | solution.py:108
  46.4 0.0 copy-done.3
  46.4 3.6 %collective-permute-start = (bf16[2,512]{1,0:T(2,128)(2,1)S(1)}, bf16[2,512]{1,0:T(2,128)(2,1)S(1)}, u32[]{:S(2)}, u32[]{:S(2)}) collective-permute-start(bf16[2,512]{1,0:T(2,128)(2,1)S(1)} %slice.43), channel_id=1, source_target_pairs={{0,4},{4,8},{8,12},{12,16},{16,20},{20,24},{24,28},{28,32},{32,36}... | collective-permute-start | bytes 6152 | tf_op jit(solution)/shard_map/ppermute | solution.py:12
  50.0 0.0 copy-done.4
  50.0 2.1 collective-permute-start.1
  52.1 0.0 copy-start.8
  52.1 0.8 dynamic-slice_convert_fusion
  52.9 12.1 %all-gather.1 = bf16[128,2048]{1,0:T(8,128)(2,1)S(1)} all-gather(bf16[32,2048]{1,0:T(8,128)(2,1)S(1)} %get-tuple-element.5), channel_id=3, replica_groups=mesh['grp'=2,'ep'=32,'tp'=4] {'tp'}, dimensions={0}, use_global_device_ids=true | all-gather | bytes 655360 | tf_op jit(solution)/shard_map/all_gather | solution.py:28
  65.0 11.9 %all-gather = bf16[128,2048]{1,0:T(8,128)(2,1)S(1)} all-gather(bf16[32,2048]{1,0:T(8,128)(2,1)S(1)} %get-tuple-element.4), channel_id=2, replica_groups=mesh['grp'=2,'ep'=32,'tp'=4] {'tp'}, dimensions={0}, use_global_device_ids=true | all-gather | bytes 655360 | tf_op jit(solution)/shard_map/all_gather | solution.py:28
  76.9 0.0 copy-done.1
  76.9 0.3 fusion.31
  77.2 0.3 fusion.33
  77.5 0.0 copy-done.8
  77.5 0.3 fusion.12
  77.8 0.0 copy-start.7
  77.8 0.0 copy-start.9
  77.8 0.3 fusion.11
  78.1 0.0 copy-done.2
  78.1 0.4 convolution_convert_fusion.1
  78.5 33.7 %collective-permute-done = bf16[2,512]{1,0:T(2,128)(2,1)S(1)} collective-permute-done((bf16[2,512]{1,0:T(2,128)(2,1)S(1)}, bf16[2,512]{1,0:T(2,128)(2,1)S(1)}, u32[]{:S(2)}, u32[]{:S(2)}) %collective-permute-start) | collective-permute-done | bytes 2080 | tf_op jit(solution)/shard_map/ppermute | solution.py:12
  112.2 0.0 collective-permute-done.1
  112.3 0.1 convert_multiply_fusion.2
  112.4 0.0 copy-done.7
  112.4 0.0 copy-done.9
  112.4 0.8 convolution_convert_fusion.2
  113.2 1.5 pad_maximum_fusion
  114.8 29.5 %all-to-all-done.1 = bf16[128,3,2048]{2,1,0:T(4,128)(2,1)} async-done(((bf16[128,3,2048]{2,1,0:T(4,128)(2,1)}), bf16[128,3,2048]{2,1,0:T(4,128)(2,1)}, u32[]{:S(2)}, u32[]{:S(2)}) %all-to-all-start.1) | async-done | bytes 1572896 | tf_op jit(solution)/shard_map/all_to_all | solution.py:108
  144.3 4.7 %all-to-all-start = ((bf16[4,64,4096]{2,1,0:T(8,128)(2,1)}), bf16[4,64,4096]{2,1,0:T(8,128)(2,1)}, u32[]{:S(2)}, u32[]{:S(2)}) async-start(bf16[4,64,4096]{2,1,0:T(8,128)(2,1)} %pad_maximum_fusion), calls=%async_computation | async-start | bytes 4194304 | tf_op jit(solution)/shard_map/all_to_all | solution.py:40
  149.0 5.1 %reshape.99 = bf16[384,2048]{1,0:T(8,128)(2,1)} reshape(bf16[128,3,2048]{2,1,0:T(4,128)(2,1)} %all-to-all-done.1) | data formatting | bytes 3145728 | tf_op jit(solution)/shard_map/reshape | solution.py:109
  154.1 3.0 %fusion.3 = f32[384,512]{1,0:T(8,128)S(1)} fusion(bf16[384,2048]{1,0:T(8,128)(2,1)} %reshape.99, bf16[1,2048,512]{2,1,0:T(8,128)(2,1)} %param.26), kind=kOutput, calls=%fused_computation.11 | convolution fusion | flops 805306368 | bytes 4456448 | tf_op jit(solution)/shard_map/dot_general | solution.py:110
  157.1 0.0 copy-done
  157.1 5.2 %convolution_convert_fusion = bf16[384,2048]{1,0:T(8,128)(2,1)} fusion(bf16[1,512,2048]{2,1,0:T(8,128)(2,1)S(1)} %copy-done, bf16[384,2048]{1,0:T(8,128)(2,1)} %reshape.99, bf16[1,2048,512]{2,1,0:T(8,128)(2,1)} %param.27, f32[384,512]{1,0:T(8,128)S(1)} %fusion.3), kind=kOutput, calls=%fused_computation.4 | convolution fusion | flops 1612578816 | bytes 8126464 | tf_op jit(solution)/shard_map/dot_general | solution.py:113
  162.3 5.2 %reshape.100 = bf16[128,3,2048]{2,1,0:T(4,128)(2,1)} reshape(bf16[384,2048]{1,0:T(8,128)(2,1)} %convolution_convert_fusion) | data formatting | bytes 3145728 | tf_op jit(solution)/shard_map/reshape | solution.py:117
  167.5 7.3 %all-to-all-done = bf16[4,64,4096]{2,1,0:T(8,128)(2,1)} async-done(((bf16[4,64,4096]{2,1,0:T(8,128)(2,1)}), bf16[4,64,4096]{2,1,0:T(8,128)(2,1)}, u32[]{:S(2)}, u32[]{:S(2)}) %all-to-all-start) | async-done | bytes 2097184 | tf_op jit(solution)/shard_map/all_to_all | solution.py:40
  174.8 10.2 %all-to-all-start.2 = ((bf16[128,3,2048]{2,1,0:T(4,128)(2,1)}), bf16[128,3,2048]{2,1,0:T(4,128)(2,1)}, u32[]{:S(2)}, u32[]{:S(2)}) async-start(bf16[128,3,2048]{2,1,0:T(4,128)(2,1)} %reshape.100), calls=%async_computation.2 | async-start | bytes 4194304 | tf_op jit(solution)/shard_map/all_to_all | solution.py:116
  185.1 0.0 copy-done.6
  185.1 0.1 copy.19
  185.2 2.0 convert_reduce_fusion
  187.2 0.1 multiply_reduce_fusion.1
  187.4 95.6 %all-to-all-done.2 = bf16[128,3,2048]{2,1,0:T(4,128)(2,1)} async-done(((bf16[128,3,2048]{2,1,0:T(4,128)(2,1)}), bf16[128,3,2048]{2,1,0:T(4,128)(2,1)}, u32[]{:S(2)}, u32[]{:S(2)}) %all-to-all-start.2) | async-done | bytes 1572896 | tf_op jit(solution)/shard_map/all_to_all | solution.py:116
  283.0 5.0 %reshape.101 = bf16[384,2048]{1,0:T(8,128)(2,1)} reshape(bf16[128,3,2048]{2,1,0:T(4,128)(2,1)} %all-to-all-done.2) | data formatting | bytes 3145728 | tf_op jit(solution)/shard_map/reshape | solution.py:123
  288.0 5.0 %gather_fusion.1 = bf16[256,2048]{1,0:T(8,128)(2,1)} fusion(bf16[384,2048]{1,0:T(8,128)(2,1)} %reshape.101, s32[1024]{0:T(1024)S(1)} %pad_clamp_fusion), kind=kCustom, calls=%fused_computation.1 | custom fusion | bytes 2098176 | tf_op jit(solution)/shard_map/gather | solution.py:123
  293.0 2.7 reshape.102
  295.7 3.2 %multiply_reduce_fusion = f32[64,2048]{1,0:T(8,128)S(1)} fusion(f32[64,4,2048]{2,1,0:T(4,128)} %reshape.102, f32[64,4]{1,0:T(8,128)S(1)} %copy.19), kind=kLoop, calls=%fused_computation.13 | loop fusion | flops 917504 | bytes 2622464 | tf_op jit(solution)/shard_map/reduce_sum | solution.py:125
  298.9 0.0 copy-done.5
  298.9 0.9 fusion.23
  (20 shorter events, 0.2 us)
Async XLA Ops:
  0.6 156.5 %copy-start = (bf16[1,512,2048]{2,1,0:T(8,128)(2,1)S(1)}, bf16[1,512,2048]{2,1,0:T(8,128)(2,1)}, u32[]{:S(2)}) copy-start(bf16[1,512,2048]{2,1,0:T(8,128)(2,1)} %param.28) | copy-start | bytes 6291460
  15.2 31.2 %copy-start.3 = (bf16[256,512]{1,0:T(8,128)(2,1)S(1)}, bf16[256,512]{1,0:T(8,128)(2,1)}, u32[]{:S(2)}) copy-start(bf16[256,512]{1,0:T(8,128)(2,1)} %param.17) | copy-start | bytes 786436
  15.2 34.8 %copy-start.4 = (bf16[256,512]{1,0:T(8,128)(2,1)S(1)}, bf16[256,512]{1,0:T(8,128)(2,1)}, u32[]{:S(2)}) copy-start(bf16[256,512]{1,0:T(8,128)(2,1)} %param.18) | copy-start | bytes 786436
  15.2 61.7 %copy-start.1 = (bf16[2048,128]{1,0:T(8,128)(2,1)S(1)}, bf16[2048,128]{1,0:T(8,128)(2,1)}, u32[]{:S(2)}) copy-start(bf16[2048,128]{1,0:T(8,128)(2,1)} %param.29) | copy-start | bytes 1572868
  15.2 129.1 %all-to-all-start.1 = ((bf16[128,3,2048]{2,1,0:T(4,128)(2,1)}), bf16[128,3,2048]{2,1,0:T(4,128)(2,1)}, u32[]{:S(2)}, u32[]{:S(2)}) async-start(bf16[128,3,2048]{2,1,0:T(4,128)(2,1)} %reshape.98), calls=%async_computation.1 | async-start | bytes 4194304 | tf_op jit(solution)/shard_map/all_to_all | solution.py:108
  46.4 65.8 %collective-permute-start = (bf16[2,512]{1,0:T(2,128)(2,1)S(1)}, bf16[2,512]{1,0:T(2,128)(2,1)S(1)}, u32[]{:S(2)}, u32[]{:S(2)}) collective-permute-start(bf16[2,512]{1,0:T(2,128)(2,1)S(1)} %slice.43), channel_id=1, source_target_pairs={{0,4},{4,8},{8,12},{12,16},{16,20},{20,24},{24,28},{28,32},{32,36}... | collective-permute-start | bytes 6152 | tf_op jit(solution)/shard_map/ppermute | solution.py:12
  50.0 62.3 %collective-permute-start.1 = (bf16[2,512]{1,0:T(2,128)(2,1)S(1)}, bf16[2,512]{1,0:T(2,128)(2,1)S(1)}, u32[]{:S(2)}, u32[]{:S(2)}) collective-permute-start(bf16[2,512]{1,0:T(2,128)(2,1)S(1)} %slice.44), channel_id=1, source_target_pairs={{0,4},{4,8},{8,12},{12,16},{16,20},{20,24},{24,28},{28,32},{32,36}... | collective-permute-start | bytes 6152 | tf_op jit(solution)/shard_map/ppermute | solution.py:12
  52.1 25.4 %copy-start.8 = (bf16[2048,128]{1,0:T(8,128)(2,1)S(1)}, bf16[2048,128]{1,0:T(8,128)(2,1)}, u32[]{:S(2)}) copy-start(bf16[2048,128]{1,0:T(8,128)(2,1)} %param.30) | copy-start | bytes 1572868
  76.9 1.2 copy-start.2
  77.8 34.6 %copy-start.7 = (bf16[512,2048]{1,0:T(8,128)(2,1)S(1)}, bf16[512,2048]{1,0:T(8,128)(2,1)}, u32[]{:S(2)}) copy-start(bf16[512,2048]{1,0:T(8,128)(2,1)} %param.20) | copy-start | bytes 6291460
  77.8 34.6 %copy-start.9 = (bf16[256,512]{1,0:T(8,128)(2,1)S(1)}, bf16[256,512]{1,0:T(8,128)(2,1)}, u32[]{:S(2)}) copy-start(bf16[256,512]{1,0:T(8,128)(2,1)} %param.16) | copy-start | bytes 786436
  144.3 30.5 %all-to-all-start = ((bf16[4,64,4096]{2,1,0:T(8,128)(2,1)}), bf16[4,64,4096]{2,1,0:T(8,128)(2,1)}, u32[]{:S(2)}, u32[]{:S(2)}) async-start(bf16[4,64,4096]{2,1,0:T(8,128)(2,1)} %pad_maximum_fusion), calls=%async_computation | async-start | bytes 4194304 | tf_op jit(solution)/shard_map/all_to_all | solution.py:40
  167.5 17.6 %copy-start.6 = (f32[64,4]{0,1:T(4,128)S(1)}, f32[64,4]{0,1:T(4,128)}, u32[]{:S(2)}) copy-start(f32[64,4]{0,1:T(4,128)} %param.25) | copy-start | bytes 3076
  174.8 108.2 %all-to-all-start.2 = ((bf16[128,3,2048]{2,1,0:T(4,128)(2,1)}), bf16[128,3,2048]{2,1,0:T(4,128)(2,1)}, u32[]{:S(2)}, u32[]{:S(2)}) async-start(bf16[128,3,2048]{2,1,0:T(4,128)(2,1)} %reshape.100), calls=%async_computation.2 | async-start | bytes 4194304 | tf_op jit(solution)/shard_map/all_to_all | solution.py:116
  295.7 3.2 %copy-start.5 = (f32[2048]{0:T(1024)S(1)}, f32[2048]{0:T(1024)}, u32[]{:S(2)}) copy-start(f32[2048]{0:T(1024)} %param.21) | copy-start | bytes 24580
where the time goes:
time: 301 us; the launch traced here: 300 us
  waiting for transfers between devices  166 us (55%)
  starting transfers between devices  51.8 us (17%)
  local copies, waits for them, and re-layouts  34.1 us (11%)
  blocking collectives  24 us (8%)
  other arithmetic  12.1 us (4%)
  matrix products  10.6 us (4%)
    all_to_all x1, waiting for transfers between devices, on_device(): lax.all_to_all(result.reshape(expert_count, capacity, feature_width), ('e...  95.6 us
    ppermute x2, waiting for transfers between devices, passed_along(): return lax.ppermute(array, axis, pairs)  33.7 us
    all_to_all x1, starting transfers between devices, on_device(): lax.all_to_all(outgoing, ('ep', 'tp'), split_axis=0, concat_axis=0, tiled...  31.2 us
    all_to_all x1, waiting for transfers between devices, on_device(): lax.all_to_all(outgoing, ('ep', 'tp'), split_axis=0, concat_axis=0, tiled...  29.5 us
    all_gather x2, blocking collectives, work_in_pieces(): outs.append(jax.vmap(apply)(lax.all_gather(share, axis), starts))  24 us
    all_to_all x1, starting transfers between devices, on_device(): lax.all_to_all(result.reshape(expert_count, capacity, feature_width), ('e...  10.2 us
    all_to_all x1, waiting for transfers between devices, summed_on_arrival(): lax.all_to_all(pieces, axis, split_axis=0, concat_axis=0, tiled=True)  7.35 us
  transfers between devices with their start and end apart: 5, of which 4 were waited for; matrix products, arithmetic and copies ran while one was open for 9% of the time, Pallas kernels for 0%

commit v1 on v0

--- a/solution.py
+++ b/solution.py
@@ -36,9 +36,26 @@
 
 
 def summed_on_arrival(array, axis, dim):
-    pieces = in_blocks(array, dim, lax.axis_size(axis))
-    arrived = lax.all_to_all(pieces, axis, split_axis=0, concat_axis=0, tiled=True)
-    return arrived.astype(jnp.float32).sum(axis=0)
+    size = lax.axis_size(axis)
+    pieces = in_blocks(array, dim, size)
+    own = lax.axis_index(axis)
+    total = jnp.take(pieces, own, axis=0).astype(jnp.float32)
+    for k in range(1, size):
+        going = jnp.take(pieces, (own + k) % size, axis=0)
+        total = total + lax.ppermute(
+            going, axis, [(i, (i + k) % size) for i in range(size)]
+        ).astype(jnp.float32)
+    return total
+
+
+LANES = 128
+
+
+def exchanged(rows, expert_count, capacity):
+    width = rows.shape[-1]
+    cut = rows.reshape(expert_count, capacity * width // LANES, LANES)
+    cut = lax.all_to_all(cut, ("ep", "tp"), split_axis=0, concat_axis=0, tiled=True)
+    return cut.reshape(expert_count * capacity, width)
 
 
 def rms_scale(values, gains):
@@ -104,23 +121,15 @@
     target = flat_ids * capacity + slot_rank
     token_of = jnp.arange(flat_ids.shape[0], dtype=jnp.int32) // top_count
     slot_token = jnp.zeros((expert_count * capacity,), jnp.int32).at[target].set(token_of)
-    outgoing = normed[slot_token].reshape(expert_count, capacity, feature_width)
-    arrived = lax.all_to_all(outgoing, ("ep", "tp"), split_axis=0, concat_axis=0, tiled=True)
-    flat_in = arrived.reshape(expert_count * capacity, feature_width)
+    flat_in = exchanged(normed[slot_token], expert_count, capacity)
     gate_value = jnp.dot(flat_in, expert_gate[0], preferred_element_type=jnp.float32)
     up_value = jnp.dot(flat_in, expert_up[0], preferred_element_type=jnp.float32)
     active = (jax.nn.silu(gate_value) * up_value).astype(jnp.bfloat16)
     result = jnp.dot(active, expert_down[0], preferred_element_type=jnp.float32).astype(
         jnp.bfloat16
     )
-    returned = lax.all_to_all(
-        result.reshape(expert_count, capacity, feature_width),
-        ("ep", "tp"),
-        split_axis=0,
-        concat_axis=0,
-        tiled=True,
-    )
-    picked = returned.reshape(expert_count * capacity, feature_width)[target].astype(jnp.float32)
+    returned = exchanged(result, expert_count, capacity)
+    picked = returned[target].astype(jnp.float32)
     weights = route_weights.reshape(-1)
     routed = jnp.sum(
         (weights[:, None] * picked).reshape(row_count, top_count, feature_width), axis=1

time: 301 us -> 256 us (0.85)
  the two profiles are of different devices: /device:TPU:33 before, /device:TPU:297 now
where the time goes in v1:
time: 256 us; the launch traced here: 255 us
  blocking collectives  126 us (49%)
  waiting for transfers between devices  49.5 us (19%)
  local copies, waits for them, and re-layouts  29.4 us (11%)
  starting transfers between devices  22 us (9%)
  matrix products  15.4 us (6%)
  other arithmetic  12.5 us (5%)
    all_to_all x1, blocking collectives, exchanged(): lax.all_to_all(cut, ('ep', 'tp'), split_axis=0, concat_axis=0, tiled=True)  102 us
    ppermute x2, waiting for transfers between devices, passed_along(): return lax.ppermute(array, axis, pairs)  27.3 us
    all_gather x2, blocking collectives, work_in_pieces(): outs.append(jax.vmap(apply)(lax.all_gather(share, axis), starts))  24.1 us
    ppermute x3, waiting for transfers between devices, summed_on_arrival(): lax.ppermute(going, axis, [(i, (i + k) % size) for i in range(size)])  22.2 us
    all_to_all x1, starting transfers between devices, exchanged(): lax.all_to_all(cut, ('ep', 'tp'), split_axis=0, concat_axis=0, tiled=True)  11.8 us
    reshape x2, local copies, waits for them, and re-layouts, exchanged(): cut = rows.reshape(expert_count, capacity * width // LANES, LANES)  7.52 us
    reshape x2, local copies, waits for them, and re-layouts, exchanged(): return cut.reshape(expert_count * capacity, width)  7.41 us
    ppermute x2, starting transfers between devices, passed_along(): return lax.ppermute(array, axis, pairs)  5.6 us
  transfers between devices with their start and end apart: 6, of which 4 were waited for; matrix products, arithmetic and copies ran while one was open for 5% of the time, Pallas kernels for 0%

profile of v1, /device:TPU:297, one launch (start us, length us, event | category | flops | bytes accessed | tf_op | source)
XLA Modules:
  0.0 255.4 jit_solution(14776083014437706045)
XLA Ops:
  0.6 0.0 copy-start
  0.6 0.9 copy.21
  1.6 0.1 eq.33
  1.7 0.1 eq.29
  1.8 0.7 broadcast_multiply_fusion
  2.5 1.1 fusion.20
  3.6 0.1 copy.23
  3.7 0.2 fusion.52
  4.0 0.1 copy.20
  4.1 0.1 mul.154
  4.2 0.2 fusion.54
  4.4 1.4 scatter_custom_fusion
  5.8 1.1 fusion.22
  6.9 3.1 %gather_fusion = bf16[384,2048]{1,0:T(8,128)(2,1)} fusion(bf16[64,2048]{1,0:T(8,128)(2,1)S(1)} %fusion.22, s32[1024]{0:T(1024)S(1)} %pad_clamp_fusion.1), kind=kCustom, calls=%fused_computation | custom fusion | bytes 3147264 | tf_op jit(solution)/shard_map/gather | solution.py:124
  10.1 3.8 %reshape.99 = bf16[128,48,128]{2,1,0:T(8,128)(2,1)} reshape(bf16[384,2048]{1,0:T(8,128)(2,1)} %gather_fusion) | data formatting | bytes 3145728 | tf_op jit(solution)/shard_map/reshape | solution.py:56
  13.8 101.5 %all_to_all.10 = bf16[128,48,128]{2,1,0:T(8,128)(2,1)} all-to-all(bf16[128,48,128]{2,1,0:T(8,128)(2,1)} %reshape.99), channel_id=1, replica_groups=mesh['grp'=2,'ep'=32,'tp'=4] {'ep','tp'}, dimensions={0} | all-to-all | bytes 3145728 | tf_op jit(solution)/shard_map/all_to_all | solution.py:57
  115.4 3.7 %reshape.100 = bf16[384,2048]{1,0:T(8,128)(2,1)} reshape(bf16[128,48,128]{2,1,0:T(8,128)(2,1)} %all_to_all.10) | data formatting | bytes 3145728 | tf_op jit(solution)/shard_map/reshape | solution.py:58
  119.1 3.0 %fusion.3 = f32[384,512]{1,0:T(8,128)S(1)} fusion(bf16[384,2048]{1,0:T(8,128)(2,1)} %reshape.100, bf16[1,2048,512]{2,1,0:T(8,128)(2,1)} %param.28), kind=kOutput, calls=%fused_computation.17 | convolution fusion | flops 805306368 | bytes 4456448 | tf_op jit(solution)/shard_map/dot_general | solution.py:125
  122.1 0.0 copy-done
  122.1 5.1 %convolution_convert_fusion = bf16[384,2048]{1,0:T(8,128)(2,1)} fusion(bf16[1,512,2048]{2,1,0:T(8,128)(2,1)S(1)} %copy-done, bf16[384,2048]{1,0:T(8,128)(2,1)} %reshape.100, bf16[1,2048,512]{2,1,0:T(8,128)(2,1)} %param.29, f32[384,512]{1,0:T(8,128)S(1)} %fusion.3), kind=kOutput, calls=%fused_computation.11 | convolution fusion | flops 1612578816 | bytes 8126464 | tf_op jit(solution)/shard_map/dot_general | solution.py:128
  127.3 3.8 %reshape.101 = bf16[128,48,128]{2,1,0:T(8,128)(2,1)} reshape(bf16[384,2048]{1,0:T(8,128)(2,1)} %convolution_convert_fusion) | data formatting | bytes 3145728 | tf_op jit(solution)/shard_map/reshape | solution.py:56
  131.0 11.8 %all-to-all-start.1 = ((bf16[128,48,128]{2,1,0:T(8,128)(2,1)}), bf16[128,48,128]{2,1,0:T(8,128)(2,1)}, u32[]{:S(2)}, u32[]{:S(2)}) async-start(bf16[128,48,128]{2,1,0:T(8,128)(2,1)} %reshape.101), calls=%async_computation.1 | async-start | bytes 3145728 | tf_op jit(solution)/shard_map/all_to_all | solution.py:57
  142.8 0.0 copy-done.5
  142.8 3.5 %collective-permute-start = (bf16[2,512]{1,0:T(2,128)(2,1)S(1)}, bf16[2,512]{1,0:T(2,128)(2,1)S(1)}, u32[]{:S(2)}, u32[]{:S(2)}) collective-permute-start(bf16[2,512]{1,0:T(2,128)(2,1)S(1)} %slice.43), channel_id=1, source_target_pairs={{0,4},{4,8},{8,12},{12,16},{16,20},{20,24},{24,28},{28,32},{32,36}... | collective-permute-start | bytes 6152 | tf_op jit(solution)/shard_map/ppermute | solution.py:12
  146.3 0.7 slice.44
  147.0 2.1 collective-permute-start.1
  149.2 0.7 dynamic-slice_convert_fusion
  149.9 12.2 %all-gather = bf16[128,2048]{1,0:T(8,128)(2,1)S(1)} all-gather(bf16[32,2048]{1,0:T(8,128)(2,1)S(1)} %get-tuple-element.19), channel_id=2, replica_groups=mesh['grp'=2,'ep'=32,'tp'=4] {'tp'}, dimensions={0}, use_global_device_ids=true | all-gather | bytes 655360 | tf_op jit(solution)/shard_map/all_gather | solution.py:28
  162.1 11.9 %all-gather.1 = bf16[128,2048]{1,0:T(8,128)(2,1)S(1)} all-gather(bf16[32,2048]{1,0:T(8,128)(2,1)S(1)} %get-tuple-element.20), channel_id=3, replica_groups=mesh['grp'=2,'ep'=32,'tp'=4] {'tp'}, dimensions={0}, use_global_device_ids=true | all-gather | bytes 655360 | tf_op jit(solution)/shard_map/all_gather | solution.py:28
  174.0 1.4 fusion.45
  175.4 1.3 fusion.43
  176.7 1.3 fusion.11
  178.0 0.0 copy-done.8
  178.1 0.3 fusion.12
  178.4 0.0 copy-done.4
  178.4 0.4 convolution_convert_fusion.1
  178.8 27.1 %collective-permute-done = bf16[2,512]{1,0:T(2,128)(2,1)S(1)} collective-permute-done((bf16[2,512]{1,0:T(2,128)(2,1)S(1)}, bf16[2,512]{1,0:T(2,128)(2,1)S(1)}, u32[]{:S(2)}, u32[]{:S(2)}) %collective-permute-start) | collective-permute-done | bytes 2080 | tf_op jit(solution)/shard_map/ppermute | solution.py:12
  206.0 0.1 collective-permute-done.1
  206.1 1.1 convert_multiply_fusion.2
  207.2 2.5 convolution_convert_fusion.2
  209.7 0.0 copy-start.3
  209.7 0.0 copy-start.7
  209.7 1.0 copy-done.3
  210.7 1.3 fusion.31
  212.0 1.3 collective-permute-start.2
  213.3 2.3 collective-permute-start.3
  215.6 1.1 collective-permute-start.4
  216.6 0.0 copy-done.7
  216.6 0.1 copy.19
  216.7 9.6 %collective-permute-done.2 = bf16[64,4096]{1,0:T(8,128)(2,1)} collective-permute-done((bf16[64,4096]{1,0:T(8,128)(2,1)}, bf16[64,4096]{1,0:T(8,128)(2,1)}, u32[]{:S(2)}, u32[]{:S(2)}) %collective-permute-start.2) | collective-permute-done | bytes 524320 | tf_op jit(solution)/shard_map/ppermute | solution.py:45
  226.4 12.6 %collective-permute-done.3 = bf16[64,4096]{1,0:T(8,128)(2,1)} collective-permute-done((bf16[64,4096]{1,0:T(8,128)(2,1)}, bf16[64,4096]{1,0:T(8,128)(2,1)}, u32[]{:S(2)}, u32[]{:S(2)}) %collective-permute-start.3) | collective-permute-done | bytes 524320 | tf_op jit(solution)/shard_map/ppermute | solution.py:45
  238.9 0.0 collective-permute-done.4
  238.9 1.7 convert_add_fusion
  240.6 0.0 copy-start.1
  240.6 1.0 copy-done.1
  241.6 0.1 multiply_reduce_fusion.1
  241.8 0.0 all-to-all-done.1
  241.8 3.7 %reshape.102 = bf16[384,2048]{1,0:T(8,128)(2,1)} reshape(bf16[128,48,128]{2,1,0:T(8,128)(2,1)} %all-to-all-done.1) | data formatting | bytes 3145728 | tf_op jit(solution)/shard_map/reshape | solution.py:58
  245.5 4.0 %gather_fusion.1 = bf16[256,2048]{1,0:T(8,128)(2,1)S(1)} fusion(bf16[384,2048]{1,0:T(8,128)(2,1)} %reshape.102, s32[1024]{0:T(1024)S(1)} %pad_clamp_fusion), kind=kCustom, calls=%fused_computation.1 | custom fusion | bytes 2098176 | tf_op jit(solution)/shard_map/gather | solution.py:132
  249.5 1.7 reshape.162
  251.2 3.3 %multiply_reduce_fusion = f32[64,2048]{1,0:T(8,128)S(1)} fusion(f32[64,4,2048]{2,1,0:T(4,128)} %reshape.162, f32[64,4]{1,0:T(8,128)S(1)} %copy.19), kind=kLoop, calls=%fused_computation.19 | loop fusion | flops 917504 | bytes 2622464 | tf_op jit(solution)/shard_map/reduce_sum | solution.py:134
  254.5 0.0 copy-done.2
  254.5 0.0 copy-done.6
  254.5 0.9 fusion.35
  (21 shorter events, 0.2 us)
Async XLA Ops:
  0.6 121.5 %copy-start = (bf16[1,512,2048]{2,1,0:T(8,128)(2,1)S(1)}, bf16[1,512,2048]{2,1,0:T(8,128)(2,1)}, u32[]{:S(2)}) copy-start(bf16[1,512,2048]{2,1,0:T(8,128)(2,1)} %param.30) | copy-start | bytes 6291460
  131.0 11.8 %copy-start.5 = (bf16[256,512]{1,0:T(8,128)(2,1)S(1)}, bf16[256,512]{1,0:T(8,128)(2,1)}, u32[]{:S(2)}) copy-start(bf16[256,512]{1,0:T(8,128)(2,1)} %param.19) | copy-start | bytes 786436
  131.0 110.8 %all-to-all-start.1 = ((bf16[128,48,128]{2,1,0:T(8,128)(2,1)}), bf16[128,48,128]{2,1,0:T(8,128)(2,1)}, u32[]{:S(2)}, u32[]{:S(2)}) async-start(bf16[128,48,128]{2,1,0:T(8,128)(2,1)} %reshape.101), calls=%async_computation.1 | async-start | bytes 3145728 | tf_op jit(solution)/shard_map/all_to_all | solution.py:57
  142.8 63.2 %collective-permute-start = (bf16[2,512]{1,0:T(2,128)(2,1)S(1)}, bf16[2,512]{1,0:T(2,128)(2,1)S(1)}, u32[]{:S(2)}, u32[]{:S(2)}) collective-permute-start(bf16[2,512]{1,0:T(2,128)(2,1)S(1)} %slice.43), channel_id=1, source_target_pairs={{0,4},{4,8},{8,12},{12,16},{16,20},{20,24},{24,28},{28,32},{32,36}... | collective-permute-start | bytes 6152 | tf_op jit(solution)/shard_map/ppermute | solution.py:12
  147.0 59.1 %collective-permute-start.1 = (bf16[2,512]{1,0:T(2,128)(2,1)S(1)}, bf16[2,512]{1,0:T(2,128)(2,1)S(1)}, u32[]{:S(2)}, u32[]{:S(2)}) collective-permute-start(bf16[2,512]{1,0:T(2,128)(2,1)S(1)} %slice.44), channel_id=1, source_target_pairs={{0,4},{4,8},{8,12},{12,16},{16,20},{20,24},{24,28},{28,32},{32,36}... | collective-permute-start | bytes 6152 | tf_op jit(solution)/shard_map/ppermute | solution.py:12
  162.1 16.0 %copy-start.8 = (bf16[2048,128]{1,0:T(8,128)(2,1)S(1)}, bf16[2048,128]{1,0:T(8,128)(2,1)}, u32[]{:S(2)}) copy-start(bf16[2048,128]{1,0:T(8,128)(2,1)} %param.32) | copy-start | bytes 1572868
  174.0 4.4 %copy-start.4 = (bf16[128,2048]{1,0:T(8,128)(2,1)S(1)}, bf16[128,2048]{1,0:T(8,128)(2,1)}, u32[]{:S(2)}) copy-start(bf16[128,2048]{1,0:T(8,128)(2,1)} %param.33) | copy-start | bytes 1572868
  209.7 1.0 copy-start.3
  209.7 6.9 %copy-start.7 = (f32[64,4]{0,1:T(4,128)S(1)}, f32[64,4]{0,1:T(4,128)}, u32[]{:S(2)}) copy-start(f32[64,4]{0,1:T(4,128)} %param.27) | copy-start | bytes 3076
  212.0 14.4 %collective-permute-start.2 = (bf16[64,4096]{1,0:T(8,128)(2,1)}, bf16[64,4096]{1,0:T(8,128)(2,1)}, u32[]{:S(2)}, u32[]{:S(2)}) collective-permute-start(bf16[64,4096]{1,0:T(8,128)(2,1)} %get-tuple-element.14), channel_id=1, source_target_pairs={{0,1},{1,2},{2,3},{3,0},{4,5},{5,6},{6,7},{7,4},{8,9},{9,10},{10,1... | collective-permute-start | bytes 1572872 | tf_op jit(solution)/shard_map/ppermute | solution.py:45
  213.3 25.6 %collective-permute-start.3 = (bf16[64,4096]{1,0:T(8,128)(2,1)}, bf16[64,4096]{1,0:T(8,128)(2,1)}, u32[]{:S(2)}, u32[]{:S(2)}) collective-permute-start(bf16[64,4096]{1,0:T(8,128)(2,1)} %get-tuple-element.15), channel_id=1, source_target_pairs={{0,2},{1,3},{2,0},{3,1},{4,6},{5,7},{6,4},{7,5},{8,10},{9,11},{10,... | collective-permute-start | bytes 1572872 | tf_op jit(solution)/shard_map/ppermute | solution.py:45
  215.6 23.4 %collective-permute-start.4 = (bf16[64,4096]{1,0:T(8,128)(2,1)}, bf16[64,4096]{1,0:T(8,128)(2,1)}, u32[]{:S(2)}, u32[]{:S(2)}) collective-permute-start(bf16[64,4096]{1,0:T(8,128)(2,1)} %get-tuple-element.16), channel_id=1, source_target_pairs={{0,3},{1,0},{2,1},{3,2},{4,7},{5,4},{6,5},{7,6},{8,11},{9,8},{10,9... | collective-permute-start | bytes 1572872 | tf_op jit(solution)/shard_map/ppermute | solution.py:45
  240.6 1.0 copy-start.1
  251.2 3.3 %copy-start.2 = (f32[64,4096]{1,0:T(8,128)S(1)}, f32[64,4096]{1,0:T(8,128)}, u32[]{:S(2)}) copy-start(f32[64,4096]{1,0:T(8,128)} %copy-done.1) | copy-start | bytes 3145732
  251.2 3.3 %copy-start.6 = (f32[2048]{0:T(1024)S(1)}, f32[2048]{0:T(1024)}, u32[]{:S(2)}) copy-start(f32[2048]{0:T(1024)} %param.23) | copy-start | bytes 24580
